TPU v7x, 512 devices: a 4x2x32 block of a 4x8x32 slice. The times are simulated.
512 devices in a mesh: grp: 2 (over y), sp: 64 (over z, core), tp: 4 (over x).
Axes of the slice: x: 4, y: 2, z: 32, core: 2. Of those that a mesh axis runs over, the one named last changes fastest.
The devices are a block of a 4x8x32 slice.
Arguments:
- query_latent: bfloat16 [16384, 768], P(('grp', 'sp')), parts along dimension 0, may hold values from -6 to 6
- key_latent: bfloat16 [16384, 256], P(('grp', 'sp', 'tp')), parts along dimension 0, may hold values from -20 to 20
- rotary_key: bfloat16 [16384, 64], P(('grp', 'sp', 'tp')), parts along dimension 0, may hold values from -1000 to 1000
- query_gain: float32 [768], replicated, may hold values from 0.1 to 1.9
- latent_gain: float32 [256], replicated, may hold values from 0.1 to 1.9
- query_up: bfloat16 [768, 3072], P(None, 'tp'), may hold values from -0.21875 to 0.21875
- key_up: bfloat16 [256, 2048], P(None, 'tp'), may hold values from -0.375 to 0.375
- value_up: bfloat16 [256, 2048], P(None, 'tp'), may hold values from -0.375 to 0.375
- out_gain: float32 [2048], P('tp'), may hold values from 0.1 to 1.9
- out_weight: bfloat16 [2048, 4096], P('sp', 'tp'), may hold values from -0.125 to 0.125
Outputs:
- mixed: bfloat16 [16384, 4096], P(('grp', 'sp'), 'tp'), parts along dimension 0
There are 2 independent parts, one for each index of `grp`. A program takes and returns all parts, laid end to end along the dimension named above; an argument that names none is the same for every part. Nothing has to cross between parts.
All inputs are finite; a program needn't handle non-finite values.
Results may differ from a plain program's by a relative error of at most 0.02.
The roundings to bfloat16 on the way count: a program that leaves them out, or rounds other values in their place, can miss the bound.
Values may be sent and summed in bfloat16 or wider, within the bound.
No kernel may reach another device: no remote copies, remote signals or barrier semaphores. Data moves between devices by JAX's collectives and lax.ppermute only.
A program may use at most 128 MiB of HBM per device.

v0:
```python
import jax
import jax.numpy as jnp
from jax import lax
from jax.sharding import PartitionSpec as P

HEADS = 16
NOPE_DIM = 128
ROPE_DIM = 64
VALUE_DIM = 128
KVRANK = 256
norm_eps = 1e-06
rope_theta = 10000.0


def side_by_side(arrays, axis, dim, along):
    widths = [a.shape[along] for a in arrays]
    both = jnp.concatenate(arrays, axis=along)
    filled = lax.all_gather(both, axis, axis=dim, tiled=True)
    return tuple(jnp.split(filled, [sum(widths[:k]) for k in range(1, len(widths))], axis=along))


def rms_scaled(inputs, gain_vec):
    widened = inputs.astype(jnp.float32)
    return (
        widened
        * lax.rsqrt(jnp.mean(widened * widened, axis=-1, keepdims=True) + norm_eps)
        * gain_vec
    )


def rotate_half(inputs, positions):
    half_width = inputs.shape[-1] // 2
    inverse = rope_theta ** (-jnp.arange(half_width, dtype=jnp.float32) / half_width)
    angles = positions[:, None] * inverse[None, :]
    if inputs.ndim == 3:
        angles = angles[:, None, :]
    cosine = jnp.cos(angles)
    sine = jnp.sin(angles)
    widened = inputs.astype(jnp.float32)
    first = widened[..., :half_width]
    second = widened[..., half_width:]
    return jnp.concatenate(
        [first * cosine - second * sine, second * cosine + first * sine], axis=-1
    )


def on_device(
    query_latent,
    key_latent,
    rotary_key,
    query_gain,
    latent_gain,
    query_up,
    key_up,
    value_up,
    out_gain,
    out_weight,
):
    block_rows = query_latent.shape[0]
    row_count = key_latent.shape[0]
    head_local = key_up.shape[1] // NOPE_DIM
    block_start = lax.axis_index("sp") * block_rows
    own_start = block_start + lax.axis_index("tp") * row_count
    score_scale = (NOPE_DIM + ROPE_DIM) ** (-0.5)
    normed = rms_scaled(query_latent, query_gain).astype(jnp.bfloat16)
    query_full = jnp.dot(normed, query_up, preferred_element_type=jnp.float32).astype(jnp.bfloat16)
    query_full = query_full.reshape(block_rows, head_local, NOPE_DIM + ROPE_DIM)
    query_positions = (block_start + jnp.arange(block_rows, dtype=jnp.int32)).astype(jnp.float32)
    query_plain = query_full[..., :NOPE_DIM]
    query_turned = rotate_half(query_full[..., NOPE_DIM:], query_positions).astype(jnp.bfloat16)
    latent_normed = rms_scaled(key_latent, latent_gain).astype(jnp.bfloat16)
    own_positions = (own_start + jnp.arange(row_count, dtype=jnp.int32)).astype(jnp.float32)
    key_turned = rotate_half(rotary_key, own_positions).astype(jnp.bfloat16)
    block_latents, block_keys = side_by_side((latent_normed, key_turned), "tp", 0, 1)
    running_max = jnp.full((block_rows, head_local), -1e30, jnp.float32)
    running_sum = jnp.zeros((block_rows, head_local), jnp.float32)
    weighted = jnp.zeros((block_rows, head_local, KVRANK), jnp.float32)
    latents, turned_keys = side_by_side((block_latents, block_keys), "sp", 0, 1)
    portion_rows = latents.shape[0]
    step_rows = min(portion_rows, 2048)
    for begin in range(0, portion_rows, step_rows):
        latent_part = latents[begin : begin + step_rows]
        turned_part = turned_keys[begin : begin + step_rows]
        key_plain = jnp.dot(latent_part, key_up, preferred_element_type=jnp.float32).astype(
            jnp.bfloat16
        )
        key_plain = key_plain.reshape(latent_part.shape[0], head_local, NOPE_DIM)
        scores = jnp.einsum(
            "qhd,khd->qhk", query_plain, key_plain, preferred_element_type=jnp.float32
        )
        scores = scores + jnp.einsum(
            "qhd,kd->qhk", query_turned, turned_part, preferred_element_type=jnp.float32
        )
        scores = scores * score_scale
        new_max = jnp.maximum(running_max, jnp.max(scores, axis=-1))
        rescale = jnp.exp(running_max - new_max)
        expo = jnp.exp(scores - new_max[..., None])
        running_sum = running_sum * rescale + jnp.sum(expo, axis=-1)
        weighted = weighted * rescale[..., None] + jnp.einsum(
            "qhk,kc->qhc",
            expo.astype(jnp.bfloat16),
            latent_part,
            preferred_element_type=jnp.float32,
        )
        running_max = new_max
    final_state = (running_max, running_sum, weighted)
    running_max, running_sum, weighted = final_state
    latent_mix = (weighted / running_sum[..., None]).astype(jnp.bfloat16)
    value_heads = value_up.reshape(KVRANK, head_local, VALUE_DIM)
    head_out = jnp.einsum(
        "qhc,chd->qhd", latent_mix, value_heads, preferred_element_type=jnp.float32
    ).astype(jnp.bfloat16)
    head_out = head_out.reshape(block_rows, head_local * VALUE_DIM)
    widened = head_out.astype(jnp.float32)
    square_part = jnp.sum(widened * widened, axis=1)
    gained = (widened * out_gain).astype(jnp.bfloat16)
    all_gained, square_parts = (
        lax.all_gather(gained, "tp", axis=1, tiled=True),
        lax.all_gather(square_part[:, None].astype(jnp.bfloat16), "tp", axis=1, tiled=True).astype(
            jnp.float32
        ),
    )
    all_squares = jnp.sum(square_parts, axis=1)
    own_sums = jnp.dot(
        all_gained,
        lax.all_gather(out_weight, "sp", axis=0, tiled=True),
        preferred_element_type=jnp.float32,
    )
    mean_square = all_squares / (HEADS * VALUE_DIM)
    return (own_sums * lax.rsqrt(mean_square + norm_eps)[:, None]).astype(jnp.bfloat16)


def solution(mesh):
    in_specs = (
        P(("grp", "sp"), None),
        P(("grp", "sp", "tp"), None),
        P(("grp", "sp", "tp"), None),
        P(),
        P(),
        P(None, "tp"),
        P(None, "tp"),
        P(None, "tp"),
        P("tp"),
        P("sp", "tp"),
    )
    out_specs = P(("grp", "sp"), "tp")
    return jax.shard_map(
        on_device, mesh=mesh, in_specs=in_specs, out_specs=out_specs, check_vma=False
    )
```

profile of v0, /device:TPU:33, one launch (start us, length us, event | category | flops | bytes accessed | tf_op | source)
XLA Modules:
  0.0 333.3 jit_solution(3699053288763499415)
XLA Ops:
  6.5 0.0 copy-start
  6.6 0.0 copy-start.3
  6.6 0.0 all-gather.4.cloned.1.call-start
  6.6 0.8 convert_element_type.106
  7.4 0.8 fusion.91
  8.2 0.8 fusion.93
  9.0 0.1 fusion.99
  9.2 0.1 pad_maximum_fusion.1
  9.3 10.5 %all_gather.15 = bf16[128,320]{1,0:T(8,128)(2,1)S(1)} all-gather(bf16[32,320]{1,0:T(8,128)(2,1)S(1)} %pad_maximum_fusion.1), channel_id=1, replica_groups=mesh['grp'=2,'sp'=64,'tp'=4] {'tp'}, dimensions={0}, use_global_device_ids=true | all-gather | bytes 102400 | tf_op jit(solution)/shard_map/all_gather | solution.py:18
  19.7 0.7 copy.37
  20.5 0.1 all-gather.4.cloned.1.call-update
  20.5 0.1 all-gather.6.cloned.1.call-start
  20.6 0.7 all-gather.6.cloned.1.call-update
  21.4 1.0 fusion.75
  22.4 0.0 copy-done
  22.4 1.3 convolution_convert_fusion.4
  23.7 0.2 copy.38
  23.9 0.1 multiply_cosine_fusion
  24.1 1.1 copy.77
  25.2 167.6 %all-gather.4.cloned.1.call-done = bf16[8192,320]{0,1:T(8,128)(2,1)} async-done(((bf16[128,320]{0,1:T(8,128)(2,1)}), bf16[8192,320]{0,1:T(8,128)(2,1)}) %all-gather.4.cloned.1.call-update) | async-done | bytes 5242896 | tf_op jit(solution)/shard_map/all_gather | solution.py:18
  192.8 0.0 copy-start.2
  192.8 2.2 convolution_convert_fusion.3
  195.0 0.0 copy-done.3
  195.0 2.0 convolution_convert_fusion
  196.9 0.0 copy-done.2
  197.0 0.8 convolution_convert_fusion.1
  197.7 0.8 convolution_convert_fusion.2
  198.5 0.9 fusion.87
  199.4 0.9 fusion.89
  200.3 0.9 fusion.83
  201.2 0.9 fusion.85
  202.1 0.8 fusion.108
  202.8 0.8 fusion.105
  203.6 0.0 copy-start.1
  203.6 0.8 fusion.106
  204.4 0.8 fusion.107
  205.2 1.1 fusion.4
  206.3 0.0 copy-done.1
  206.3 1.1 fusion.8
  207.4 1.0 fusion.27
  208.4 0.8 fusion.33
  209.2 0.8 fusion.39
  209.9 0.0 copy-start.4
  210.0 3.5 %multiply_reduce_fusion = (bf16[128]{0:T(256)(128)(2,1)S(1)}, f32[4,128,128]{1,2,0:T(8,128)S(1)}) fusion(bf16[256,4,128]{0,2,1:T(8,128)(2,1)S(1)} %bitcast.87, f32[128,4,256]{2,0,1:T(8,128)S(1)} %fusion.39, f32[128,4,2048]{0,2,1:T(8,128)} %copy-done.1, f32[128,4]{0,1:T(4,128)S(1)} %get-tuple-element.9, bf16[8192,320]{0,1:T(8,128)(2,1)} %all-gather.4.cloned.1.call-done, ...), kind=kOutput, calls=%fused_computation.70 | convolution fusion | flops 573177728 | bytes 6295808 | tf_op jit(solution)/shard_map/qhc,chd->qhd/dot_general | solution.py:110
  213.4 7.7 %all-gather = bf16[4,1,128]{2,1,0:T(2,128)(2,1)S(1)} all-gather(bf16[1,1,128]{2,1,0:T(2,128)(2,1)S(1)} %bitcast.88), channel_id=1, replica_groups=mesh['grp'=2,'sp'=64,'tp'=4] {'tp'}, dimensions={0}, use_global_device_ids=true | all-gather | bytes 1280 | tf_op jit(solution)/shard_map/all_gather | solution.py:119
  221.1 0.0 copy-done.4
  221.1 0.1 fusion.78
  221.3 10.5 %all_gather.17 = bf16[128,2048]{0,1:T(8,128)(2,1)S(1)} all-gather(bf16[128,512]{0,1:T(8,128)(2,1)S(1)} %fusion.78), channel_id=1, replica_groups=mesh['grp'=2,'sp'=64,'tp'=4] {'tp'}, dimensions={1}, use_global_device_ids=true | all-gather | bytes 655360 | tf_op jit(solution)/shard_map/all_gather | solution.py:118
  231.8 91.0 %all-gather.6.cloned.1.call-done = bf16[2048,1024]{1,0:T(8,128)(2,1)} async-done(((bf16[32,1024]{1,0:T(8,128)(2,1)}), bf16[2048,1024]{1,0:T(8,128)(2,1)}) %all-gather.6.cloned.1.call-update) | async-done | bytes 4194320 | tf_op jit(solution)/shard_map/all_gather | solution.py:126
  322.8 3.6 %fusion.45 = bf16[128,1024]{1,0:T(8,128)(2,1)} fusion(bf16[128,2048]{0,1:T(8,128)(2,1)S(1)} %all_gather.17, bf16[2048,1024]{1,0:T(8,128)(2,1)} %all-gather.6.cloned.1.call-done, f32[128]{0:T(128)S(1)} %add_rsqrt_fusion), kind=kOutput, calls=%fused_computation.40 | convolution fusion | flops 537133056 | bytes 4981248 | tf_op jit(solution)/shard_map/dot_general | solution.py:124
  (11 shorter events, 0.1 us)
Async XLA Ops:
  6.5 15.9 %copy-start = (bf16[768,768]{1,0:T(8,128)(2,1)S(1)}, bf16[768,768]{1,0:T(8,128)(2,1)}, u32[]{:S(2)}) copy-start(bf16[768,768]{1,0:T(8,128)(2,1)} %param.15) | copy-start | bytes 3538948
  6.6 188.4 %copy-start.3 = (bf16[256,512]{1,0:T(8,128)(2,1)S(1)}, bf16[256,512]{1,0:T(8,128)(2,1)}, u32[]{:S(2)}) copy-start(bf16[256,512]{1,0:T(8,128)(2,1)} %param.16) | copy-start | bytes 786436
  6.6 186.2 %all-gather.4.cloned.1.call-start = ((), (), s32[]{:S(2)}) async-start(), calls=%async_computation | async-start | bytes 5324800 | tf_op jit(solution)/shard_map/all_gather | solution.py:18
  20.5 302.2 %all-gather.6.cloned.1.call-start = ((), (), s32[]{:S(2)}) async-start(), calls=%async_computation.1 | async-start | bytes 4259840 | tf_op jit(solution)/shard_map/all_gather | solution.py:126
  192.8 4.2 %copy-start.2 = (bf16[8192,320]{0,1:T(8,128)(2,1)S(1)}, bf16[8192,320]{0,1:T(8,128)(2,1)}, u32[]{:S(2)}) copy-start(bf16[8192,320]{0,1:T(8,128)(2,1)} %all-gather.4.cloned.1.call-done) | copy-start | bytes 15728644
  203.6 2.7 copy-start.1
  209.9 11.2 %copy-start.4 = (f32[512]{0:T(512)S(1)}, f32[512]{0:T(512)}, u32[]{:S(2)}) copy-start(f32[512]{0:T(512)} %param.18) | copy-start | bytes 6148
Sparse Core Ops, SparseCore 0:
  20.7 172.0 all-gather.3
  194.9 127.8 all-gather.5
where the time goes:
time: 334 us; the launch traced here: 333 us
  waiting for transfers between devices  259 us (78%)
  blocking collectives  28.7 us (9%)
  matrix products  23.1 us (7%)
  between operations  13.6 us (4%)
  other arithmetic  6.34 us (2%)
    all_gather x1, waiting for transfers between devices, side_by_side(): filled = lax.all_gather(both, axis, axis=dim, tiled=True)  168 us
    all_gather x1, waiting for transfers between devices, on_device(): lax.all_gather(out_weight, 'sp', axis=0, tiled=True)  91 us
    all_gather x1, blocking collectives, on_device(): lax.all_gather(gained, 'tp', axis=1, tiled=True)  10.5 us
    all_gather x1, blocking collectives, side_by_side(): filled = lax.all_gather(both, axis, axis=dim, tiled=True)  10.5 us
    all_gather x1, blocking collectives, on_device(): lax.all_gather(square_part[:, None].astype(jnp.bfloat16), 'tp', axis=1, t...  7.7 us
  transfers between devices with their start and end apart: 2, of which 2 were waited for; matrix products, arithmetic and copies ran while one was open for 7% of the time, Pallas kernels for 0%

commit v1 on v0

--- a/solution.py
+++ b/solution.py
@@ -123,7 +123,9 @@
     all_squares = jnp.sum(square_parts, axis=1)
     own_sums = jnp.dot(
         all_gained,
-        lax.all_gather(out_weight, "sp", axis=0, tiled=True),
+        jnp.concatenate(
+            lax.all_to_all(jnp.stack([out_weight] * lax.axis_size("sp")), "sp", 0, 0), axis=0
+        ),
         preferred_element_type=jnp.float32,
     )
     mean_square = all_squares / (HEADS * VALUE_DIM)

time: 334 us -> 521 us (1.56)
  waiting for transfers between devices: 259 us -> 393 us
  starting transfers between devices: 0.07 us -> 47.7 us
    all_gather x1, waiting for transfers between devices: 168 us -> 393 us  [side_by_side(): filled = lax.all_gather(both, axis, axis=dim, tiled=True)]
    all_gather x1 -> x0, waiting for transfers between devices: 91 us -> none  [on_device(): lax.all_gather(out_weight, 'sp', axis=0, tiled=True)]
    all_to_all x0 -> x1, starting transfers between devices: none -> 47.6 us  [on_device(): lax.all_to_all(jnp.stack([out_weight] * lax.axis_size('sp')), 'sp', 0, 0)]
  transfers between devices with their start and end apart: 2 -> 2, of which waited for: 2 -> 1; matrix products, arithmetic and copies ran while one was open for 7% -> 4% of each run, Pallas kernels for 0% -> 0%
where the time goes in v1:
time: 521 us; the launch traced here: 516 us
  waiting for transfers between devices  393 us (75%)
  starting transfers between devices  47.7 us (9%)
  blocking collectives  32.2 us (6%)
  matrix products  22 us (4%)
  between operations  13.7 us (3%)
    all_gather x1, waiting for transfers between devices, side_by_side(): filled = lax.all_gather(both, axis, axis=dim, tiled=True)  393 us
    all_to_all x1, starting transfers between devices, on_device(): lax.all_to_all(jnp.stack([out_weight] * lax.axis_size('sp')), 'sp', 0, 0)  47.6 us
    all_gather x1, blocking collectives, side_by_side(): filled = lax.all_gather(both, axis, axis=dim, tiled=True)  11.2 us
    all_gather x1, blocking collectives, on_device(): lax.all_gather(square_part[:, None].astype(jnp.bfloat16), 'tp', axis=1, t...  10.8 us
  transfers between devices with their start and end apart: 2, of which 1 were waited for; matrix products, arithmetic and copies ran while one was open for 4% of the time, Pallas kernels for 0%

profile of v1, /device:TPU:33, one launch (start us, length us, event | category | flops | bytes accessed | tf_op | source)
XLA Modules:
  0.0 516.3 jit_solution(12219983268907171532)
XLA Ops:
  6.5 0.0 copy-start
  6.6 3.5 stack.2
  10.1 0.0 copy-start.7
  10.1 0.0 copy-start.6
  10.1 0.0 copy-start.10
  10.1 0.0 copy-start.4
  10.1 0.0 copy-start.8
  10.1 0.0 copy-start.5
  10.1 0.0 copy-start.3
  10.1 47.6 %all-to-all-start = ((bf16[64,32,1024]{2,1,0:T(8,128)(2,1)}), bf16[64,32,1024]{2,1,0:T(8,128)(2,1)}, u32[]{:S(2)}, u32[]{:S(2)}) async-start(bf16[64,32,1024]{2,1,0:T(8,128)(2,1)} %stack.2), calls=%async_computation | async-start | bytes 8388608 | tf_op jit(solution)/shard_map/all_to_all | solution.py:127
  57.7 0.1 all-gather.3.cloned.1.call-start
  57.8 0.0 copy-done.7
  57.9 0.0 copy-done.6
  57.9 0.1 fusion.91
  58.0 0.1 fusion.99
  58.2 0.0 copy-done.10
  58.2 0.1 fusion.93
  58.2 0.1 pad_maximum_fusion.1
  58.3 11.2 %all_gather.12 = bf16[128,320]{1,0:T(8,128)(2,1)S(1)} all-gather(bf16[32,320]{1,0:T(8,128)(2,1)S(1)} %pad_maximum_fusion.1), channel_id=1, replica_groups=mesh['grp'=2,'sp'=64,'tp'=4] {'tp'}, dimensions={0}, use_global_device_ids=true | all-gather | bytes 102400 | tf_op jit(solution)/shard_map/all_gather | solution.py:18
  69.5 0.7 copy.37
  70.2 0.1 all-gather.3.cloned.1.call-update
  70.3 0.0 copy-done.4
  70.3 0.1 fusion.75
  70.4 0.0 copy-done
  70.4 0.0 copy-done.8
  70.5 0.4 convolution_convert_fusion.4
  70.8 0.2 copy.38
  71.0 0.0 copy-done.5
  71.0 0.1 copy.77
  71.2 0.1 multiply_cosine_fusion
  71.3 392.6 %all-gather.3.cloned.1.call-done = bf16[8192,320]{0,1:T(8,128)(2,1)} async-done(((bf16[128,320]{0,1:T(8,128)(2,1)}), bf16[8192,320]{0,1:T(8,128)(2,1)}) %all-gather.3.cloned.1.call-update) | async-done | bytes 5242896 | tf_op jit(solution)/shard_map/all_gather | solution.py:18
  463.9 0.0 copy-done.3
  463.9 0.0 copy-start.2
  463.9 2.1 convolution_convert_fusion.3
  466.1 2.0 convolution_convert_fusion
  468.0 0.0 copy-done.2
  468.0 0.8 convolution_convert_fusion.1
  468.8 0.8 convolution_convert_fusion.2
  469.6 0.9 fusion.87
  470.5 0.9 fusion.89
  471.4 0.9 fusion.83
  472.3 0.9 fusion.85
  473.2 0.8 fusion.108
  473.9 0.8 fusion.105
  474.7 0.0 copy-start.1
  474.7 0.8 fusion.106
  475.5 0.8 fusion.107
  476.3 1.1 fusion.4
  477.4 0.0 copy-done.1
  477.4 1.3 fusion.8
  478.8 0.8 fusion.27
  479.5 0.8 fusion.33
  480.3 0.8 fusion.39
  481.1 0.0 copy-start.9
  481.1 3.5 multiply_reduce_fusion
  484.5 10.8 %all-gather = bf16[4,1,128]{2,1,0:T(2,128)(2,1)S(1)} all-gather(bf16[1,1,128]{2,1,0:T(2,128)(2,1)S(1)} %bitcast.89), channel_id=1, replica_groups=mesh['grp'=2,'sp'=64,'tp'=4] {'tp'}, dimensions={0}, use_global_device_ids=true | all-gather | bytes 1280 | tf_op jit(solution)/shard_map/all_gather | solution.py:119
  495.3 0.0 copy-done.9
  495.3 0.1 fusion.78
  495.5 10.3 %all_gather.14 = bf16[128,2048]{0,1:T(8,128)(2,1)S(1)} all-gather(bf16[128,512]{0,1:T(8,128)(2,1)S(1)} %fusion.78), channel_id=1, replica_groups=mesh['grp'=2,'sp'=64,'tp'=4] {'tp'}, dimensions={1}, use_global_device_ids=true | all-gather | bytes 655360 | tf_op jit(solution)/shard_map/all_gather | solution.py:118
  505.8 0.0 all-to-all-done
  505.8 3.6 fusion.45
  (12 shorter events, 0.1 us)
Async XLA Ops:
  6.5 63.9 %copy-start = (bf16[768,768]{1,0:T(8,128)(2,1)S(1)}, bf16[768,768]{1,0:T(8,128)(2,1)}, u32[]{:S(2)}) copy-start(bf16[768,768]{1,0:T(8,128)(2,1)} %param.15) | copy-start | bytes 3538948
  10.1 47.7 %copy-start.7 = (bf16[32,64]{1,0:T(8,128)(2,1)S(1)}, bf16[32,64]{1,0:T(8,128)(2,1)}, u32[]{:S(2)}) copy-start(bf16[32,64]{1,0:T(8,128)(2,1)} %param.12) | copy-start | bytes 12292
  10.1 47.8 %copy-start.6 = (bf16[32,256]{1,0:T(8,128)(2,1)S(1)}, bf16[32,256]{1,0:T(8,128)(2,1)}, u32[]{:S(2)}) copy-start(bf16[32,256]{1,0:T(8,128)(2,1)} %param.11) | copy-start | bytes 49156
  10.1 48.1 %copy-start.10 = (f32[256]{0:T(256)S(1)}, f32[256]{0:T(256)}, u32[]{:S(2)}) copy-start(f32[256]{0:T(256)} %param.14) | copy-start | bytes 3076
  10.1 60.2 %copy-start.4 = (bf16[128,768]{1,0:T(8,128)(2,1)S(1)}, bf16[128,768]{1,0:T(8,128)(2,1)}, u32[]{:S(2)}) copy-start(bf16[128,768]{1,0:T(8,128)(2,1)} %param.10) | copy-start | bytes 589828
  10.1 60.4 %copy-start.8 = (f32[768]{0:T(1024)S(1)}, f32[768]{0:T(1024)}, u32[]{:S(2)}) copy-start(f32[768]{0:T(1024)} %param.13) | copy-start | bytes 9220
  10.1 60.9 %copy-start.5 = (bf16[256,512]{1,0:T(8,128)(2,1)S(1)}, bf16[256,512]{1,0:T(8,128)(2,1)}, u32[]{:S(2)}) copy-start(bf16[256,512]{1,0:T(8,128)(2,1)} %param.17) | copy-start | bytes 786436
  10.1 453.8 %copy-start.3 = (bf16[256,512]{1,0:T(8,128)(2,1)S(1)}, bf16[256,512]{1,0:T(8,128)(2,1)}, u32[]{:S(2)}) copy-start(bf16[256,512]{1,0:T(8,128)(2,1)} %param.16) | copy-start | bytes 786436
  10.1 495.6 %all-to-all-start = ((bf16[64,32,1024]{2,1,0:T(8,128)(2,1)}), bf16[64,32,1024]{2,1,0:T(8,128)(2,1)}, u32[]{:S(2)}, u32[]{:S(2)}) async-start(bf16[64,32,1024]{2,1,0:T(8,128)(2,1)} %stack.2), calls=%async_computation | async-start | bytes 8388608 | tf_op jit(solution)/shard_map/all_to_all | solution.py:127
  57.7 406.2 %all-gather.3.cloned.1.call-start = ((), (), s32[]{:S(2)}) async-start(), calls=%async_computation.1 | async-start | bytes 5324800 | tf_op jit(solution)/shard_map/all_gather | solution.py:18
  463.9 4.1 copy-start.2
  474.7 2.7 copy-start.1
  481.1 14.3 %copy-start.9 = (f32[512]{0:T(512)S(1)}, f32[512]{0:T(512)}, u32[]{:S(2)}) copy-start(f32[512]{0:T(512)} %param.18) | copy-start | bytes 6148
Sparse Core Ops, SparseCore 0:
  70.4 393.4 all-gather.2
